TPU v7x, 512 devices: a whole 4x8x8 slice. The times are simulated.
512 devices in a mesh: sp: 32 (over z, x), tp: 16 (over y, core).
Axes of the slice: x: 4, y: 8, z: 8, core: 2. Of those that a mesh axis runs over, the one named last changes fastest.
Arguments:
- hidden_in: bfloat16 [2, 49152, 2048], P(None, ('sp', 'tp')), may hold values from -6 to 6
- w_value: bfloat16 [2048, 2048], P(None, 'tp'), may hold values from -0.125 to 0.125
- w_key: bfloat16 [2048, 2048], P(None, 'tp'), may hold values from -0.125 to 0.125
- w_step: bfloat16 [2048, 32], replicated, may hold values from -0.125 to 0.125
- conv_value: bfloat16 [4, 2048], P(None, 'tp'), may hold values from -3 to 3
- conv_key: bfloat16 [4, 2048], P(None, 'tp'), may hold values from -3 to 3
- step_bias: float32 [32], P('tp'), may hold values from -3 to -1
- decay_rate: float32 [32], P('tp'), may hold values from 2.03450521e-06 to 0.25
- decay_jump: float32 [2, 49152, 32], P(None, 'sp', 'tp'), may hold values from -0.75 to 0
- new_value: bfloat16 [2, 2048], P(None, 'tp'), may hold values from -60 to 60
- new_key: bfloat16 [2, 2048], P(None, 'tp'), may hold values from -6 to 6
- new_query: bfloat16 [2, 2048], P(None, 'tp'), may hold values from -6 to 6
- new_gate: bfloat16 [2, 2048], P(None, 'tp'), may hold values from -6 to 6
- new_step: float32 [2, 32], P(None, 'tp'), may hold values from -6 to 6
- read_gain: bfloat16 [2048], P('tp'), may hold values from 0.099609375 to 1.8984375
Outputs:
- prompt_state: bfloat16 [2, 32, 64, 128], P(None, 'tp', 'sp')
- read_out: bfloat16 [2, 32, 64], P(None, 'tp', 'sp')
All inputs are finite; a program needn't handle non-finite values.
Results may differ from a plain program's by a relative error of at most 0.006.
Values may be sent and summed in bfloat16 or wider, within the bound.
No kernel may reach another device: no remote copies, remote signals or barrier semaphores. Data moves between devices by JAX's collectives and lax.ppermute only.
A program may use at most 64 MiB of HBM per device.

v0:
```python
import jax
import jax.numpy as jnp
from jax import lax
from jax.sharding import PartitionSpec as P

HEAD_DIM = 64
STATE = 128
EPSILON = 1e-05


def shifted(value, axis, steps):
    count = lax.axis_size(axis)
    leading, last = (max(0, -steps), min(count, count - steps))
    return lax.ppermute(value, axis, [(source, source + steps) for source in range(leading, last)])


def sent_to_all(shard, axis):
    length = lax.axis_size(axis)
    return lax.all_to_all(
        jnp.broadcast_to(shard[None], (length, *shard.shape)), axis, 0, 0, tiled=True
    )


def taken_together(shard, axis):
    everything = sent_to_all(shard, axis)
    return jnp.sum(everything, axis=0)


def causal_mix(padded_rows, conv_taps):
    tap_count = conv_taps.shape[0]
    length = padded_rows.shape[-2] - tap_count + 1
    running = jnp.zeros(padded_rows.shape[:-2] + (length, padded_rows.shape[-1]), jnp.float32)
    for tap_index in range(tap_count):
        running = running + padded_rows[..., tap_index : tap_index + length, :].astype(
            jnp.float32
        ) * conv_taps[tap_index].astype(jnp.float32)
    return running


def block_states(mixed_rows, weight, value_cols, groups_dev):
    seq_count, row_count, heads_dev = weight.shape
    per_group = heads_dev // groups_dev
    values = (
        mixed_rows[:, :, :value_cols].reshape(seq_count, row_count, groups_dev, per_group, HEAD_DIM)
        * weight.reshape(seq_count, row_count, groups_dev, per_group)[..., None]
    )
    keys = mixed_rows[:, :, value_cols:].reshape(seq_count, row_count, groups_dev, STATE)
    states = jnp.einsum("slgep,slgn->sgepn", values, keys, precision=lax.Precision.HIGHEST)
    return states.reshape(seq_count, heads_dev, HEAD_DIM, STATE)


def per_device(
    hidden_in,
    w_value,
    w_key,
    w_step,
    conv_value,
    conv_key,
    step_bias,
    decay_rate,
    decay_jump,
    new_value,
    new_key,
    new_query,
    new_gate,
    new_step,
    read_gain,
):
    sp_count = lax.axis_size("sp")
    sp_index = lax.axis_index("sp")
    tp_index = lax.axis_index("tp")
    heads_dev = step_bias.shape[0]
    value_cols = w_value.shape[1]
    key_cols = w_key.shape[1]
    groups_dev = key_cols // STATE
    per_group = heads_dev // groups_dev
    kernel_taps = conv_value.shape[0]
    seq_count = hidden_in.shape[0]
    share = HEAD_DIM // sp_count
    own_step = lax.dynamic_slice_in_dim(w_step, tp_index * heads_dev, heads_dev, 1)
    w_joined = jnp.concatenate([w_value, w_key, own_step], axis=1)
    projected = jnp.einsum(
        "tfy,yz->tfz",
        lax.all_gather(hidden_in, "tp", axis=1, tiled=True),
        w_joined,
        preferred_element_type=jnp.float32,
    ).astype(jnp.bfloat16)
    seg_rows = projected.shape[1]
    proj_pair = projected[:, :, : value_cols + key_cols]
    proj_step = projected[:, :, value_cols + key_cols :]
    step_size = jax.nn.softplus(proj_step.astype(jnp.float32) + step_bias)
    log_decay = decay_jump - decay_rate * step_size
    conv_taps = jnp.concatenate([conv_value, conv_key], axis=1)
    edge_rows = shifted(proj_pair[:, seg_rows - (kernel_taps - 1) :, :], "sp", 1)
    mixed_rows = jax.nn.silu(causal_mix(jnp.concatenate([edge_rows, proj_pair], axis=1), conv_taps))
    seg_total = jnp.sum(log_decay, axis=1)
    decay_after = seg_total[:, None, :] - jnp.cumsum(log_decay, axis=1)
    seg_states = block_states(mixed_rows, step_size * jnp.exp(decay_after), value_cols, groups_dev)
    tiled_totals = jnp.broadcast_to(
        seg_total[:, None, :, None], (seq_count, 1, heads_dev, sp_count)
    )
    got_states, got_totals = (
        lax.all_to_all(seg_states[:, None], "sp", split_axis=3, concat_axis=1, tiled=True),
        lax.all_to_all(tiled_totals, "sp", split_axis=3, concat_axis=1, tiled=True),
    )
    got_totals = got_totals[..., 0]
    tail_decay = jnp.sum(got_totals, axis=1, keepdims=True) - jnp.cumsum(got_totals, axis=1)
    final_state = jnp.einsum(
        "sjh,sjhpn->shpn", jnp.exp(tail_decay), got_states, precision=lax.Precision.HIGHEST
    )
    cache_state = final_state.astype(jnp.bfloat16)
    new_size = jax.nn.softplus(new_step + step_bias)
    keep_share = jnp.exp(-decay_rate * new_size)
    query = new_query.astype(jnp.float32).reshape(seq_count, groups_dev, STATE)
    own_key = new_key.astype(jnp.float32).reshape(seq_count, groups_dev, STATE)
    key_match = jnp.sum(own_key * query, axis=-1)
    size_grid = new_size.reshape(seq_count, groups_dev, per_group)
    keep_grid = keep_share.reshape(seq_count, groups_dev, per_group)
    value_grid = new_value.astype(jnp.float32).reshape(seq_count, groups_dev, per_group, HEAD_DIM)
    gate_grid = jax.nn.silu(new_gate.astype(jnp.float32)).reshape(
        seq_count, groups_dev, per_group, HEAD_DIM
    )
    gain_grid = read_gain.astype(jnp.float32).reshape(groups_dev, per_group, HEAD_DIM)
    own_value = lax.dynamic_slice_in_dim(value_grid, sp_index * share, share, 3)
    own_gate = lax.dynamic_slice_in_dim(gate_grid, sp_index * share, share, 3)
    own_gain = lax.dynamic_slice_in_dim(gain_grid, sp_index * share, share, 2)
    state_read = jnp.einsum(
        "sgepn,sgn->sgep",
        final_state.reshape(seq_count, groups_dev, per_group, share, STATE),
        query,
        precision=lax.Precision.HIGHEST,
    )
    raw_read = (
        keep_grid[..., None] * state_read
        + size_grid[..., None] * own_value * key_match[:, :, None, None]
    )
    gated = raw_read * own_gate
    squares = taken_together(jnp.sum(gated * gated, axis=(2, 3)), "sp")
    scale = lax.rsqrt(squares / (per_group * HEAD_DIM) + EPSILON)
    read_out = (gated * scale[:, :, None, None] * own_gain).astype(jnp.bfloat16)
    return (cache_state, read_out.reshape(seq_count, heads_dev, share))


def solution(mesh):
    return jax.shard_map(
        per_device,
        mesh=mesh,
        in_specs=(
            P(None, ("sp", "tp"), None),
            P(None, "tp"),
            P(None, "tp"),
            P(),
            P(None, "tp"),
            P(None, "tp"),
            P("tp"),
            P("tp"),
            P(None, "sp", "tp"),
            P(None, "tp"),
            P(None, "tp"),
            P(None, "tp"),
            P(None, "tp"),
            P(None, "tp"),
            P("tp"),
        ),
        out_specs=(P(None, "tp", "sp", None), P(None, "tp", "sp")),
        check_vma=False,
    )
```

profile of v0, /device:TPU:24, one launch (start us, length us, event | category | flops | bytes accessed | tf_op | source)
XLA Modules:
  0.0 168.7 jit_solution(7346045088244292500)
XLA Ops:
  7.2 0.7 all-gather.2.cloned.1.call-update
  7.9 1.2 copy.25
  9.2 1.2 copy.26
  11.1 0.7 convert_multiply_fusion
  11.8 0.7 reshape.141
  12.6 0.7 reshape.143
  13.3 0.7 constant_dynamic-update-slice_fusion.1
  14.0 0.7 constant_dynamic-update-slice_fusion
  14.7 0.8 multiply_reduce_fusion.1
  15.5 0.7 multiply_exponential_fusion
  16.3 75.9 %all-gather.2.cloned.1.call-done = bf16[2,1536,2048]{2,1,0:T(8,128)(2,1)} async-done(((bf16[2,96,2048]{2,1,0:T(8,128)(2,1)}), bf16[2,1536,2048]{2,1,0:T(8,128)(2,1)}) %all-gather.2.cloned.1.call-update) | async-done | bytes 12582928 | tf_op jit(solution)/shard_map/all_gather | solution.py:84
  92.2 8.1 %fusion = bf16[2,1536,258]{1,2,0:T(8,128)(2,1)S(1)} fusion(bf16[2,1536,2048]{2,1,0:T(8,128)(2,1)} %all-gather.2.cloned.1.call-done, bf16[2048,2]{0,1:T(2,128)(2,1)S(1)} %constant_dynamic-slice_fusion, bf16[2048,128]{0,1:T(8,128)(2,1)S(1)} %copy.26, bf16[2048,128]{0,1:T(8,128)(2,1)S(1)} %copy.25), kind=kOutput, calls=%fused_computation.2 | convolution fusion | flops 3250354176 | bytes 15224832 | tf_op jit(solution)/shard_map/tfy,yz->tfz/dot_general | solution.py:82
  100.3 0.7 slice.58
  101.3 1.2 reduce-window.6
  103.1 3.4 %collective-permute-start = (bf16[2,3,256]{1,2,0:T(8,128)(2,1)}, bf16[2,3,256]{1,2,0:T(8,128)(2,1)S(1)}, u32[]{:S(2)}, u32[]{:S(2)}) collective-permute-start(bf16[2,3,256]{1,2,0:T(8,128)(2,1)} %slice.58), channel_id=1, source_target_pairs={{0,16},{16,32},{32,48},{48,64},{64,80},{80,96},{96,112},{112,128},... | collective-permute-start | bytes 9224 | tf_op jit(solution)/shard_map/ppermute | solution.py:14
  107.1 9.9 %all-to-all-start = ((f32[2,1,2,32]{2,0,1,3:T(2,128)}), f32[2,1,2,32]{2,0,1,3:T(2,128)S(1)}, u32[]{:S(2)}, u32[]{:S(2)}) async-start(f32[2,1,2,32]{2,0,1,3:T(2,128)} %broadcast_in_dim.4), calls=%async_computation | async-start | bytes 65536 | tf_op jit(solution)/shard_map/all_to_all | solution.py:104
  117.3 9.5 %all-to-all-done = f32[2,1,2,32]{2,0,1,3:T(2,128)S(1)} async-done(((f32[2,1,2,32]{2,0,1,3:T(2,128)}), f32[2,1,2,32]{2,0,1,3:T(2,128)S(1)}, u32[]{:S(2)}, u32[]{:S(2)}) %all-to-all-start) | async-done | bytes 544 | tf_op jit(solution)/shard_map/all_to_all | solution.py:104
  126.9 2.6 %divide_multiply_fusion = f32[2,1536,256]{1,2,0:T(8,128)S(1)} fusion(bf16[2,1536,256]{1,2,0:T(8,128)(2,1)S(1)} %slice.59, bf16[2,3,256]{1,2,0:T(8,128)(2,1)S(1)} %collective-permute-done, f32[256]{0:T(256)S(1)} %bitcast.61, f32[256]{0:T(256)S(1)} %bitcast.62, f32[256]{0:T(256)S(1)} %bitcast.63, f32[256]{0:T(256)S(1)} %bitcast.60), kind=kLoop, calls=%fused_computation | loop fusion | flops 18874368 | bytes 4725760 | tf_op jit(solution)/shard_map/jit(silu)/mul | solution.py:95
  129.7 1.7 fusion.5
  131.3 0.7 copy.30
  132.1 3.9 %all-to-all-start.1 = ((f32[2,1,2,64,128]{4,2,0,1,3:T(2,128)}), f32[2,1,2,64,128]{4,2,0,1,3:T(2,128)S(1)}, u32[]{:S(2)}, u32[]{:S(2)}) async-start(f32[2,1,2,64,128]{4,2,0,1,3:T(2,128)} %copy.30), calls=%async_computation.1 | async-start | bytes 262144 | tf_op jit(solution)/shard_map/all_to_all | solution.py:103
  136.2 10.3 %all-to-all-done.1 = f32[2,1,2,64,128]{4,2,0,1,3:T(2,128)S(1)} async-done(((f32[2,1,2,64,128]{4,2,0,1,3:T(2,128)}), f32[2,1,2,64,128]{4,2,0,1,3:T(2,128)S(1)}, u32[]{:S(2)}, u32[]{:S(2)}) %all-to-all-start.1) | async-done | bytes 131104 | tf_op jit(solution)/shard_map/all_to_all | solution.py:103
  147.7 3.9 %all-to-all-start.2 = ((f32[32,2,1]{1,2,0:T(1,128)}), f32[32,2,1]{1,2,0:T(1,128)S(1)}, u32[]{:S(2)}, u32[]{:S(2)}) async-start(f32[32,2,1]{1,2,0:T(1,128)} %broadcast_in_dim.5), calls=%async_computation.2 | async-start | bytes 32768 | tf_op jit(solution)/shard_map/all_to_all | solution.py:19
  152.2 8.9 %all-to-all-done.2 = f32[32,2,1]{1,2,0:T(1,128)S(1)} async-done(((f32[32,2,1]{1,2,0:T(1,128)}), f32[32,2,1]{1,2,0:T(1,128)S(1)}, u32[]{:S(2)}, u32[]{:S(2)}) %all-to-all-start.2) | async-done | bytes 288 | tf_op jit(solution)/shard_map/all_to_all | solution.py:19
  (41 shorter events, 5.6 us)
Async XLA Ops:
  7.2 9.0 %copy-start = (bf16[2048,32]{0,1:T(8,128)(2,1)S(1)}, bf16[2048,32]{0,1:T(8,128)(2,1)}, u32[]{:S(2)}) copy-start(bf16[2048,32]{0,1:T(8,128)(2,1)} %param.18) | copy-start | bytes 393220
  7.2 85.0 %all-gather.2.cloned.1.call-start = ((), (), s32[]{:S(2)}) async-start(), calls=%async_computation.3 | async-start | bytes 13369344 | tf_op jit(solution)/shard_map/all_gather | solution.py:84
  16.2 84.9 %copy-start.1 = (f32[2,1536,2]{1,2,0:T(2,128)S(1)}, f32[2,1536,2]{1,2,0:T(2,128)}, u32[]{:S(2)}) copy-start(f32[2,1536,2]{1,2,0:T(2,128)} %param.23) | copy-start | bytes 73732
  16.2 84.8 %copy-start.2 = (f32[2]{0:T(128)S(1)}, f32[2]{0:T(128)}, u32[]{:S(2)}) copy-start(f32[2]{0:T(128)} %param.21) | copy-start | bytes 28
  16.2 84.8 %copy-start.3 = (f32[2]{0:T(128)S(1)}, f32[2]{0:T(128)}, u32[]{:S(2)}) copy-start(f32[2]{0:T(128)} %param.22) | copy-start | bytes 28
  103.1 23.8 %collective-permute-start = (bf16[2,3,256]{1,2,0:T(8,128)(2,1)}, bf16[2,3,256]{1,2,0:T(8,128)(2,1)S(1)}, u32[]{:S(2)}, u32[]{:S(2)}) collective-permute-start(bf16[2,3,256]{1,2,0:T(8,128)(2,1)} %slice.58), channel_id=1, source_target_pairs={{0,16},{16,32},{32,48},{48,64},{64,80},{80,96},{96,112},{112,128},... | collective-permute-start | bytes 9224 | tf_op jit(solution)/shard_map/ppermute | solution.py:14
  107.1 19.7 %all-to-all-start = ((f32[2,1,2,32]{2,0,1,3:T(2,128)}), f32[2,1,2,32]{2,0,1,3:T(2,128)S(1)}, u32[]{:S(2)}, u32[]{:S(2)}) async-start(f32[2,1,2,32]{2,0,1,3:T(2,128)} %broadcast_in_dim.4), calls=%async_computation | async-start | bytes 65536 | tf_op jit(solution)/shard_map/all_to_all | solution.py:104
  129.5 17.1 %copy-start.4 = (bf16[2,128]{1,0:T(2,128)(2,1)S(1)}, bf16[2,128]{1,0:T(2,128)(2,1)}, u32[]{:S(2)}) copy-start(bf16[2,128]{1,0:T(2,128)(2,1)} %param.26) | copy-start | bytes 1540
  132.1 14.4 %all-to-all-start.1 = ((f32[2,1,2,64,128]{4,2,0,1,3:T(2,128)}), f32[2,1,2,64,128]{4,2,0,1,3:T(2,128)S(1)}, u32[]{:S(2)}, u32[]{:S(2)}) async-start(f32[2,1,2,64,128]{4,2,0,1,3:T(2,128)} %copy.30), calls=%async_computation.1 | async-start | bytes 262144 | tf_op jit(solution)/shard_map/all_to_all | solution.py:103
  147.7 13.5 %all-to-all-start.2 = ((f32[32,2,1]{1,2,0:T(1,128)}), f32[32,2,1]{1,2,0:T(1,128)S(1)}, u32[]{:S(2)}, u32[]{:S(2)}) async-start(f32[32,2,1]{1,2,0:T(1,128)} %broadcast_in_dim.5), calls=%async_computation.2 | async-start | bytes 32768 | tf_op jit(solution)/shard_map/all_to_all | solution.py:19
Sparse Core Ops, SparseCore 0:
  10.1 82.0 all-gather.1
where the time goes:
time: 169 us
  waiting for transfers between devices  105 us (62%)
  starting transfers between devices  21 us (12%)
  between operations  14.2 us (8%)
  matrix products  10.2 us (6%)
  other arithmetic  9.05 us (5%)
  local copies, waits for them, and re-layouts  8.84 us (5%)
    all_gather x1, waiting for transfers between devices, per_device(): lax.all_gather(hidden_in, 'tp', axis=1, tiled=True)  75.9 us
    all_to_all x1, waiting for transfers between devices, per_device(): lax.all_to_all(seg_states[:, None], 'sp', split_axis=3, concat_axis=1, ti...  10.3 us
    all_to_all x1, starting transfers between devices, per_device(): lax.all_to_all(tiled_totals, 'sp', split_axis=3, concat_axis=1, tiled=True)  9.89 us
    all_to_all x1, waiting for transfers between devices, per_device(): lax.all_to_all(tiled_totals, 'sp', split_axis=3, concat_axis=1, tiled=True)  9.54 us
    all_to_all x1, waiting for transfers between devices, sent_to_all(): lax.all_to_all(jnp.broadcast_to(shard[None], (length, *shard.shape)), axi...  8.94 us
    dot_general x1, matrix products, per_device(): jnp.einsum('tfy,yz->tfz', lax.all_gather(hidden_in, 'tp', axis=1, tiled=T...  8.12 us
    all_to_all x1, starting transfers between devices, per_device(): lax.all_to_all(seg_states[:, None], 'sp', split_axis=3, concat_axis=1, ti...  3.85 us
    all_to_all x1, starting transfers between devices, sent_to_all(): lax.all_to_all(jnp.broadcast_to(shard[None], (length, *shard.shape)), axi...  3.85 us
  transfers between devices with their start and end apart: 5, of which 4 were waited for; matrix products, arithmetic and copies ran while one was open for 6% of the time, Pallas kernels for 0%

commit v1 on v0

--- a/solution.py
+++ b/solution.py
@@ -6,6 +6,13 @@
 HEAD_DIM = 64
 STATE = 128
 EPSILON = 1e-05
+
+
+def exchange_gather(x, axis, dim):
+    size = lax.axis_size(axis)
+    pieces = jnp.stack([x for _ in range(size)])
+    pieces = lax.all_to_all(pieces, axis, split_axis=0, concat_axis=0)
+    return jnp.concatenate(pieces, axis=dim)
 
 
 def shifted(value, axis, steps):
@@ -81,7 +88,7 @@
     w_joined = jnp.concatenate([w_value, w_key, own_step], axis=1)
     projected = jnp.einsum(
         "tfy,yz->tfz",
-        lax.all_gather(hidden_in, "tp", axis=1, tiled=True),
+        exchange_gather(hidden_in, "tp", 1),
         w_joined,
         preferred_element_type=jnp.float32,
     ).astype(jnp.bfloat16)

time: 169 us -> 372 us (2.20)
  waiting for transfers between devices: 105 us -> 295 us
  starting transfers between devices: 21 us -> 36 us
  local copies, waits for them, and re-layouts: 8.84 us -> 22.2 us
  between operations: 14.2 us -> 0.94 us
    all_to_all x0 -> x1, waiting for transfers between devices: none -> 272 us  [exchange_gather(): pieces = lax.all_to_all(pieces, axis, split_axis=0, concat_axis=0)]
    all_gather x1 -> x0, waiting for transfers between devices: 75.9 us -> none  [per_device(): lax.all_gather(hidden_in, 'tp', axis=1, tiled=True)]
    reshape x1 -> x2, local copies, waits for them, and re-layouts: 0.02 us -> 10.7 us  [the longest x1 10.7 us: exchange_gather(): return jnp.concatenate(pieces, axis=dim)]
    all_to_all x0 -> x1, starting transfers between devices: none -> 10.4 us  [exchange_gather(): pieces = lax.all_to_all(pieces, axis, split_axis=0, concat_axis=0)]
    another operation x1 -> x2, local copies, waits for them, and re-layouts: 0.02 us -> 7.27 us  [the longest x1 7.25 us: exchange_gather(): pieces = jnp.stack([x for _ in range(size)])]
    all_to_all x1, waiting for transfers between devices: 9.54 us -> 4 us  [per_device(): lax.all_to_all(tiled_totals, 'sp', split_axis=3, concat_axis=1, tiled=True)]
    all_to_all x1, starting transfers between devices: 3.85 us -> 7.87 us  [per_device(): lax.all_to_all(seg_states[:, None], 'sp', split_axis=3, concat_axis=1, ti...]
  transfers between devices with their start and end apart: 5 -> 5, of which waited for: 4 -> 4; matrix products, arithmetic and copies ran while one was open for 6% -> 1% of each run, Pallas kernels for 0% -> 0%
where the time goes in v1:
time: 372 us
  waiting for transfers between devices  295 us (79%)
  starting transfers between devices  36 us (10%)
  local copies, waits for them, and re-layouts  22.2 us (6%)
  matrix products  10.2 us (3%)
  other arithmetic  6.9 us (2%)
    all_to_all x1, waiting for transfers between devices, exchange_gather(): pieces = lax.all_to_all(pieces, axis, split_axis=0, concat_axis=0)  272 us
    reshape x1, local copies, waits for them, and re-layouts, exchange_gather(): return jnp.concatenate(pieces, axis=dim)  10.7 us
    all_to_all x1, starting transfers between devices, exchange_gather(): pieces = lax.all_to_all(pieces, axis, split_axis=0, concat_axis=0)  10.4 us
    all_to_all x1, waiting for transfers between devices, per_device(): lax.all_to_all(seg_states[:, None], 'sp', split_axis=3, concat_axis=1, ti...  10.3 us
    all_to_all x1, starting transfers between devices, per_device(): lax.all_to_all(tiled_totals, 'sp', split_axis=3, concat_axis=1, tiled=True)  10.2 us
    all_to_all x1, waiting for transfers between devices, sent_to_all(): lax.all_to_all(jnp.broadcast_to(shard[None], (length, *shard.shape)), axi...  8.94 us
    dot_general x1, matrix products, per_device(): jnp.einsum('tfy,yz->tfz', exchange_gather(hidden_in, 'tp', 1), w_joined,...  8.13 us
    all_to_all x1, starting transfers between devices, per_device(): lax.all_to_all(seg_states[:, None], 'sp', split_axis=3, concat_axis=1, ti...  7.87 us
  transfers between devices with their start and end apart: 5, of which 4 were waited for; matrix products, arithmetic and copies ran while one was open for 1% of the time, Pallas kernels for 0%

profile of v1, /device:TPU:24, one launch (start us, length us, event | category | flops | bytes accessed | tf_op | source)
XLA Modules:
  0.0 371.5 jit_solution(16428580625698088242)
XLA Ops:
  0.6 7.3 %stack.2 = bf16[16,2,96,2048]{3,2,1,0:T(8,128)(2,1)} broadcast(bf16[2,96,2048]{2,1,0:T(8,128)(2,1)} %param.15), dimensions={1,2,3} | broadcast | bytes 13369344 | tf_op jit(solution)/shard_map/stack | solution.py:13
  8.0 10.4 %all-to-all-start = ((bf16[16,2,96,2048]{3,2,1,0:T(8,128)(2,1)}), bf16[16,2,96,2048]{3,2,1,0:T(8,128)(2,1)}, u32[]{:S(2)}, u32[]{:S(2)}) async-start(bf16[16,2,96,2048]{3,2,1,0:T(8,128)(2,1)} %stack.2), calls=%async_computation | async-start | bytes 25165824 | tf_op jit(solution)/shard_map/all_to_all | solution.py:14
  19.2 0.6 multiply_reduce_fusion.1
  19.9 272.0 %all-to-all-done = bf16[16,2,96,2048]{3,2,1,0:T(8,128)(2,1)} async-done(((bf16[16,2,96,2048]{3,2,1,0:T(8,128)(2,1)}), bf16[16,2,96,2048]{3,2,1,0:T(8,128)(2,1)}, u32[]{:S(2)}, u32[]{:S(2)}) %all-to-all-start) | async-done | bytes 12582944 | tf_op jit(solution)/shard_map/all_to_all | solution.py:14
  292.0 10.7 %copy.27 = bf16[2,16,96,2048]{3,2,1,0:T(8,128)(2,1)} copy(bf16[2,16,96,2048]{3,2,0,1:T(8,128)(2,1)} %bitcast.1) | data formatting | bytes 25165824 | tf_op jit(solution)/shard_map/reshape | solution.py:15
  302.7 8.1 %fusion = bf16[2,1536,258]{1,2,0:T(8,128)(2,1)S(1)} fusion(bf16[2,1536,2048]{2,1,0:T(8,128)(2,1)} %bitcast.55, bf16[2048,2]{0,1:T(2,128)(2,1)S(1)} %constant_dynamic-slice_fusion, bf16[2048,128]{0,1:T(8,128)(2,1)S(1)} %copy.26, bf16[2048,128]{0,1:T(8,128)(2,1)S(1)} %copy.25), kind=kOutput, calls=%fused_computation.2 | convolution fusion | flops 3250354176 | bytes 15224832 | tf_op jit(solution)/shard_map/tfy,yz->tfz/dot_general | solution.py:89
  310.8 0.8 slice.58
  311.6 0.2 fusion.23
  311.8 0.6 broadcast_in_dim.4
  312.4 10.2 %all-to-all-start.1 = ((f32[2,1,2,32]{2,0,1,3:T(2,128)}), f32[2,1,2,32]{2,0,1,3:T(2,128)S(1)}, u32[]{:S(2)}, u32[]{:S(2)}) async-start(f32[2,1,2,32]{2,0,1,3:T(2,128)} %broadcast_in_dim.4), calls=%async_computation.1 | async-start | bytes 65536 | tf_op jit(solution)/shard_map/all_to_all | solution.py:111
  322.7 3.7 collective-permute-start
  326.4 1.2 reduce-window.6
  327.7 0.4 reduce-window.9
  328.5 4.0 %all-to-all-done.1 = f32[2,1,2,32]{2,0,1,3:T(2,128)S(1)} async-done(((f32[2,1,2,32]{2,0,1,3:T(2,128)}), f32[2,1,2,32]{2,0,1,3:T(2,128)S(1)}, u32[]{:S(2)}, u32[]{:S(2)}) %all-to-all-start.1) | async-done | bytes 544 | tf_op jit(solution)/shard_map/all_to_all | solution.py:111
  332.6 2.6 divide_multiply_fusion
  335.3 1.7 fusion.5
  337.0 0.7 copy.31
  337.7 7.9 %all-to-all-start.2 = ((f32[2,1,2,64,128]{4,2,0,1,3:T(2,128)}), f32[2,1,2,64,128]{4,2,0,1,3:T(2,128)S(1)}, u32[]{:S(2)}, u32[]{:S(2)}) async-start(f32[2,1,2,64,128]{4,2,0,1,3:T(2,128)} %copy.31), calls=%async_computation.2 | async-start | bytes 262144 | tf_op jit(solution)/shard_map/all_to_all | solution.py:110
  345.8 10.3 %all-to-all-done.2 = f32[2,1,2,64,128]{4,2,0,1,3:T(2,128)S(1)} async-done(((f32[2,1,2,64,128]{4,2,0,1,3:T(2,128)}), f32[2,1,2,64,128]{4,2,0,1,3:T(2,128)S(1)}, u32[]{:S(2)}, u32[]{:S(2)}) %all-to-all-start.2) | async-done | bytes 131104 | tf_op jit(solution)/shard_map/all_to_all | solution.py:110
  356.7 0.6 broadcast_in_dim.5
  357.3 3.8 %all-to-all-start.3 = ((f32[32,2,1]{1,2,0:T(1,128)}), f32[32,2,1]{1,2,0:T(1,128)S(1)}, u32[]{:S(2)}, u32[]{:S(2)}) async-start(f32[32,2,1]{1,2,0:T(1,128)} %broadcast_in_dim.5), calls=%async_computation.3 | async-start | bytes 32768 | tf_op jit(solution)/shard_map/all_to_all | solution.py:26
  361.3 0.6 convert_element_type.93
  361.9 8.9 %all-to-all-done.3 = f32[32,2,1]{1,2,0:T(1,128)S(1)} async-done(((f32[32,2,1]{1,2,0:T(1,128)}), f32[32,2,1]{1,2,0:T(1,128)S(1)}, u32[]{:S(2)}, u32[]{:S(2)}) %all-to-all-start.3) | async-done | bytes 288 | tf_op jit(solution)/shard_map/all_to_all | solution.py:26
  370.9 0.6 fusion.18
  (64 shorter events, 2.5 us)
Async XLA Ops:
  0.6 19.3 %copy-start = (bf16[2048,32]{0,1:T(8,128)(2,1)S(1)}, bf16[2048,32]{0,1:T(8,128)(2,1)}, u32[]{:S(2)}) copy-start(bf16[2048,32]{0,1:T(8,128)(2,1)} %param.18) | copy-start | bytes 393220
  7.9 10.5 %copy-start.1 = (bf16[2048,128]{1,0:T(8,128)(2,1)S(1)}, bf16[2048,128]{1,0:T(8,128)(2,1)}, u32[]{:S(2)}) copy-start(bf16[2048,128]{1,0:T(8,128)(2,1)} %param.17) | copy-start | bytes 1572868
  7.9 10.8 %copy-start.2 = (bf16[2048,128]{1,0:T(8,128)(2,1)S(1)}, bf16[2048,128]{1,0:T(8,128)(2,1)}, u32[]{:S(2)}) copy-start(bf16[2048,128]{1,0:T(8,128)(2,1)} %param.16) | copy-start | bytes 1572868
  7.9 11.0 %copy-start.11 = (bf16[128]{0:T(256)(128)(2,1)S(1)}, bf16[128]{0:T(256)(128)(2,1)}, u32[]{:S(2)}) copy-start(bf16[128]{0:T(256)(128)(2,1)} %param.29) | copy-start | bytes 772
  7.9 11.1 %copy-start.12 = (bf16[2,128]{1,0:T(2,128)(2,1)S(1)}, bf16[2,128]{1,0:T(2,128)(2,1)}, u32[]{:S(2)}) copy-start(bf16[2,128]{1,0:T(2,128)(2,1)} %param.27) | copy-start | bytes 1540
  7.9 11.2 %copy-start.9 = (bf16[2,128]{1,0:T(2,128)(2,1)S(1)}, bf16[2,128]{1,0:T(2,128)(2,1)}, u32[]{:S(2)}) copy-start(bf16[2,128]{1,0:T(2,128)(2,1)} %param.24) | copy-start | bytes 1540
  7.9 11.2 %copy-start.8 = (f32[2]{0:T(128)S(1)}, f32[2]{0:T(128)}, u32[]{:S(2)}) copy-start(f32[2]{0:T(128)} %param.22) | copy-start | bytes 28
  7.9 11.2 %copy-start.5 = (bf16[4,128]{1,0:T(4,128)(2,1)S(1)}, bf16[4,128]{1,0:T(4,128)(2,1)}, u32[]{:S(2)}) copy-start(bf16[4,128]{1,0:T(4,128)(2,1)} %param.19) | copy-start | bytes 3076
  7.9 11.2 %copy-start.6 = (bf16[4,128]{1,0:T(4,128)(2,1)S(1)}, bf16[4,128]{1,0:T(4,128)(2,1)}, u32[]{:S(2)}) copy-start(bf16[4,128]{1,0:T(4,128)(2,1)} %param.20) | copy-start | bytes 3076
  8.0 11.3 %copy-start.13 = (bf16[2,128]{1,0:T(2,128)(2,1)S(1)}, bf16[2,128]{1,0:T(2,128)(2,1)}, u32[]{:S(2)}) copy-start(bf16[2,128]{1,0:T(2,128)(2,1)} %param.25) | copy-start | bytes 1540
  8.0 11.2 %copy-start.14 = (bf16[2,128]{1,0:T(2,128)(2,1)S(1)}, bf16[2,128]{1,0:T(2,128)(2,1)}, u32[]{:S(2)}) copy-start(bf16[2,128]{1,0:T(2,128)(2,1)} %param.26) | copy-start | bytes 1540
  8.0 11.9 %copy-start.4 = (f32[2]{0:T(128)S(1)}, f32[2]{0:T(128)}, u32[]{:S(2)}) copy-start(f32[2]{0:T(128)} %param.21) | copy-start | bytes 28
  8.0 11.9 %copy-start.7 = (f32[2,2]{1,0:T(2,128)S(1)}, f32[2,2]{1,0:T(2,128)}, u32[]{:S(2)}) copy-start(f32[2,2]{1,0:T(2,128)} %param.28) | copy-start | bytes 52
  8.0 284.0 %all-to-all-start = ((bf16[16,2,96,2048]{3,2,1,0:T(8,128)(2,1)}), bf16[16,2,96,2048]{3,2,1,0:T(8,128)(2,1)}, u32[]{:S(2)}, u32[]{:S(2)}) async-start(bf16[16,2,96,2048]{3,2,1,0:T(8,128)(2,1)} %stack.2), calls=%async_computation | async-start | bytes 25165824 | tf_op jit(solution)/shard_map/all_to_all | solution.py:14
  302.7 8.9 %copy-start.3 = (f32[2,1536,2]{1,2,0:T(2,128)S(1)}, f32[2,1536,2]{1,2,0:T(2,128)}, u32[]{:S(2)}) copy-start(f32[2,1536,2]{1,2,0:T(2,128)} %param.23) | copy-start | bytes 73732
  312.4 20.0 %all-to-all-start.1 = ((f32[2,1,2,32]{2,0,1,3:T(2,128)}), f32[2,1,2,32]{2,0,1,3:T(2,128)S(1)}, u32[]{:S(2)}, u32[]{:S(2)}) async-start(f32[2,1,2,32]{2,0,1,3:T(2,128)} %broadcast_in_dim.4), calls=%async_computation.1 | async-start | bytes 65536 | tf_op jit(solution)/shard_map/all_to_all | solution.py:111
  322.7 9.9 %collective-permute-start = (bf16[2,3,256]{1,2,0:T(8,128)(2,1)}, bf16[2,3,256]{1,2,0:T(8,128)(2,1)S(1)}, u32[]{:S(2)}, u32[]{:S(2)}) collective-permute-start(bf16[2,3,256]{1,2,0:T(8,128)(2,1)} %slice.58), channel_id=1, source_target_pairs={{0,16},{16,32},{32,48},{48,64},{64,80},{80,96},{96,112},{112,128},... | collective-permute-start | bytes 9224 | tf_op jit(solution)/shard_map/ppermute | solution.py:21
  335.2 21.2 %copy-start.15 = (bf16[2,128]{1,0:T(2,128)(2,1)S(1)}, bf16[2,128]{1,0:T(2,128)(2,1)}, u32[]{:S(2)}) copy-start(bf16[2,128]{1,0:T(2,128)(2,1)} %param.26) | copy-start | bytes 1540
  335.2 21.4 %copy-start.10 = (f32[2]{0:T(128)S(1)}, f32[2]{0:T(128)}, u32[]{:S(2)}) copy-start(f32[2]{0:T(128)} %multiply_reduce_fusion.1) | copy-start | bytes 28
  337.7 18.4 %all-to-all-start.2 = ((f32[2,1,2,64,128]{4,2,0,1,3:T(2,128)}), f32[2,1,2,64,128]{4,2,0,1,3:T(2,128)S(1)}, u32[]{:S(2)}, u32[]{:S(2)}) async-start(f32[2,1,2,64,128]{4,2,0,1,3:T(2,128)} %copy.31), calls=%async_computation.2 | async-start | bytes 262144 | tf_op jit(solution)/shard_map/all_to_all | solution.py:110
  357.3 13.4 %all-to-all-start.3 = ((f32[32,2,1]{1,2,0:T(1,128)}), f32[32,2,1]{1,2,0:T(1,128)S(1)}, u32[]{:S(2)}, u32[]{:S(2)}) async-start(f32[32,2,1]{1,2,0:T(1,128)} %broadcast_in_dim.5), calls=%async_computation.3 | async-start | bytes 32768 | tf_op jit(solution)/shard_map/all_to_all | solution.py:26
